TPU v7x, 32 devices: a whole 2x2x4 slice. The times are simulated.
32 devices in a mesh: ep: 8 (over z, x), tp: 4 (over y, core).
Axes of the slice: x: 2, y: 2, z: 4, core: 2. Of those that a mesh axis runs over, the one named last changes fastest.
Arguments:
- pool_input: bfloat16 [4096, 1024], P('ep', 'tp'), may hold values from -6 to 6
- group_weight: bfloat16 [4, 256, 256], P('tp'), may hold values from -0.375 to 0.375
- pool_scale: float32 [1024], P('tp'), may hold values from 0.1 to 1.9
- out_weight: bfloat16 [1024, 2048], P('tp'), may hold values from -0.1875 to 0.1875
- mix_gain: float32 [2048], replicated, may hold values from 0.1 to 1.9
- expert_input: bfloat16 [8192, 2048], P(('ep', 'tp')), may hold values from -6 to 6
- routes: int32 [8192, 2], P('ep'), may hold values from 0 to 15, all different within a row; in each aligned block of 256 rows (0 to 255, 256 to 511, ...) at most 40 rows name the same one
- route_weights: float32 [8192, 2], P('ep'), may hold values from 0.2 to 2.5
- moe_in_gain: float32 [2048], replicated, may hold values from 0.1 to 1.9
- gate_weight: bfloat16 [16, 2048, 1024], P('ep', None, 'tp'), may hold values from -0.125 to 0.125
- up_weight: bfloat16 [16, 2048, 1024], P('ep', None, 'tp'), may hold values from -0.125 to 0.125
- down_weight: bfloat16 [16, 1024, 2048], P('ep', 'tp'), may hold values from -0.1875 to 0.1875
- moe_out_gain: float32 [2048], replicated, may hold values from 0.1 to 1.9
Outputs:
- mixer_out: bfloat16 [4096, 2048], P(('ep', 'tp'))
- moe_out: bfloat16 [8192, 2048], P(('ep', 'tp'))
Inputs may be any that keep to these rules, and one draw needn't show every extreme that they name: `routes`: each row names 2 different experts. In each aligned block of 256 rows no expert is named by more than 40 rows, a bound that some block reaches.
All inputs are finite; a program needn't handle non-finite values.
Results may differ from a plain program's by a relative error of at most 0.013.
Values may be sent and summed in bfloat16 or wider, within the bound.
A program may use at most 128 MiB of HBM per device.

v0:
```python
import jax
import jax.numpy as jnp
from jax import lax
from jax.sharding import PartitionSpec as P

NORM_EPS = 1e-06


def passed_along(value, axis, steps):
    count = lax.axis_size(axis)
    initial, last = (max(0, -steps), min(count, count - steps))
    return lax.ppermute(value, axis, [(source, source + steps) for source in range(initial, last)])


def rms_scale(values, gain_vec):
    mean_sq = jnp.mean(values * values, axis=-1, keepdims=True)
    return values * lax.rsqrt(mean_sq + NORM_EPS) * gain_vec


def slot_numbers(route_block, experts, capacity):
    flat_routes = route_block.reshape(-1)
    one_hot = (flat_routes[:, None] == jnp.arange(experts, dtype=jnp.int32)[None, :]).astype(
        jnp.int32
    )
    slot_rank = jnp.sum((jnp.cumsum(one_hot, axis=0) - one_hot) * one_hot, axis=1)
    return flat_routes * capacity + slot_rank


def fill_table(slot_ids, payload, empty_value, slots_total):
    return jnp.full((slots_total,), empty_value, payload.dtype).at[slot_ids].set(payload)


def on_device(
    pool_input,
    group_weight,
    pool_scale,
    out_weight,
    mix_gain,
    expert_input,
    routes,
    route_weights,
    moe_in_gain,
    gate_weight,
    up_weight,
    down_weight,
    moe_out_gain,
):
    tp_size = lax.axis_size("tp")
    ep_size = lax.axis_size("ep")
    tp_index = lax.axis_index("tp")
    rows_a = pool_input.shape[0]
    model_width = out_weight.shape[1]
    history_rows = 2**tp_size
    window = jnp.left_shift(jnp.int32(2), tp_index)
    history = passed_along(pool_input[rows_a - history_rows :], "ep", 1)
    extended = jnp.concatenate([history, pool_input], axis=0).astype(jnp.float32)
    running = jnp.cumsum(extended, axis=0)
    lagged = lax.dynamic_slice_in_dim(running, history_rows - window, rows_a, 0)
    current = running[history_rows:]
    position = lax.axis_index("ep") * rows_a + jnp.arange(rows_a, dtype=jnp.int32)
    divisor = jnp.minimum(position + 1, window).astype(jnp.float32)[:, None]
    pooled = ((current - lagged) / divisor - extended[history_rows:]).astype(jnp.bfloat16)
    grouped = (
        jnp.dot(pooled, group_weight[0], preferred_element_type=jnp.float32) * pool_scale
    ).astype(jnp.bfloat16)
    exp_dev = gate_weight.shape[0]
    experts = exp_dev * ep_size
    tok_dev = expert_input.shape[0]
    top_count = routes.shape[1]
    capacity = max(2, 5 * tok_dev * top_count // (4 * experts))
    slots_total = experts * capacity
    normed = rms_scale(expert_input.astype(jnp.float32), moe_in_gain).astype(jnp.bfloat16)
    own_routes = lax.dynamic_slice_in_dim(routes, tp_index * tok_dev, tok_dev, 0)
    own_slots = slot_numbers(own_routes, experts, capacity)
    pair_token = jnp.arange(tok_dev * top_count, dtype=jnp.int32) // top_count
    token_table = fill_table(own_slots, pair_token, tok_dev, slots_total)
    padded_rows = jnp.concatenate([normed, jnp.zeros((1, model_width), jnp.bfloat16)], axis=0)
    outgoing = padded_rows[token_table].reshape(ep_size, exp_dev * capacity, model_width)
    arrived = lax.all_to_all(outgoing, "ep", split_axis=0, concat_axis=0, tiled=True)
    received = lax.all_gather(arrived[None], "tp", axis=0, tiled=True)
    per_quarter = ep_size * exp_dev * capacity
    flat_in = received.reshape(tp_size * per_quarter, model_width)
    projected = lax.psum_scatter(
        jnp.dot(grouped, out_weight, preferred_element_type=jnp.float32).astype(jnp.bfloat16),
        "tp",
        scatter_dimension=0,
        tiled=True,
    ).astype(jnp.float32)
    piece_rows = flat_in
    piece_rows = piece_rows.reshape(
        per_quarter * lax.axis_size("tp") // (exp_dev * capacity), exp_dev, capacity, model_width
    )
    gate_act = jnp.einsum(
        "nxcd,xdf->nxcf", piece_rows, gate_weight, preferred_element_type=jnp.float32
    )
    up_act = jnp.einsum("nxcd,xdf->nxcf", piece_rows, up_weight, preferred_element_type=jnp.float32)
    hidden = (jax.nn.silu(gate_act) * up_act).astype(jnp.bfloat16)
    down_act = jnp.einsum("nxcf,xfd->nxcd", hidden, down_weight, preferred_element_type=jnp.float32)
    expert_sum = lax.psum_scatter(
        down_act.reshape(per_quarter * lax.axis_size("tp"), model_width).astype(jnp.bfloat16),
        "tp",
        scatter_dimension=0,
        tiled=True,
    )
    mixer_out = rms_scale(projected, mix_gain).astype(jnp.bfloat16)
    expert_back = expert_sum.reshape(ep_size, exp_dev * capacity, model_width)
    returned = lax.all_to_all(expert_back, "ep", split_axis=0, concat_axis=0, tiled=True)
    picked = returned.reshape(slots_total, model_width)[own_slots].reshape(
        tok_dev, top_count, model_width
    )
    own_weights = lax.dynamic_slice_in_dim(route_weights, tp_index * tok_dev, tok_dev, 0)
    combined = jnp.sum(picked.astype(jnp.float32) * own_weights[:, :, None], axis=1)
    moe_out = rms_scale(combined, moe_out_gain).astype(jnp.bfloat16)
    return (mixer_out, moe_out)


def solution(mesh):
    in_specs = (
        P("ep", "tp"),
        P("tp", None, None),
        P("tp"),
        P("tp", None),
        P(),
        P(("ep", "tp"), None),
        P("ep", None),
        P("ep", None),
        P(),
        P("ep", None, "tp"),
        P("ep", None, "tp"),
        P("ep", "tp", None),
        P(),
    )
    out_specs = (P(("ep", "tp"), None), P(("ep", "tp"), None))
    return jax.shard_map(
        on_device, mesh=mesh, in_specs=in_specs, out_specs=out_specs, check_vma=False
    )
```

profile of v0, /device:TPU:0, one launch (start us, length us, event | category | flops | bytes accessed | tf_op | source)
XLA Modules:
  0.0 366.8 jit_solution(5897632833309299964)
XLA Ops:
  7.2 0.0 copy-start
  7.2 0.0 copy-start.2
  7.2 0.0 all-gather.3.cloned.1.call-start
  7.2 0.9 broadcast_multiply_fusion
  8.1 0.1 copy.29
  8.3 0.1 eq.29
  8.4 0.1 eq.25
  8.6 1.2 reduce-window.16
  9.7 0.2 slice_reduce_fusion
  10.0 0.1 copy.28
  10.1 0.1 mul.122
  10.3 0.1 fusion.41
  10.4 2.4 scatter_custom_fusion
  12.9 1.5 fusion.8
  14.4 0.0 copy-done.2
  14.4 1.0 fusion.10
  15.4 0.1 concatenate.7
  15.5 4.1 %gather_fusion = bf16[640,2048]{1,0:T(8,128)(2,1)} fusion(bf16[257,2048]{1,0:T(8,128)(2,1)S(1)} %concatenate.7, s32[1024]{0:T(1024)S(1)} %pad_clamp_fusion.1), kind=kCustom, calls=%fused_computation | custom fusion | bytes 5245440 | tf_op jit(solution)/shard_map/gather | solution.py:78
  19.6 66.9 %all_to_all.10 = bf16[8,80,2048]{2,1,0:T(8,128)(2,1)} all-to-all(bf16[8,80,2048]{2,1,0:T(8,128)(2,1)} %bitcast.84), channel_id=1, replica_groups=mesh['ep'=8,'tp'=4] {'ep'}, dimensions={0} | all-to-all | bytes 5242880 | tf_op jit(solution)/shard_map/all_to_all | solution.py:79
  86.4 0.0 all-gather.3.cloned.1.call-update
  86.5 0.2 reduce-scatter.5.cloned.1.call-start
  86.7 69.1 %all-gather.3.cloned.1.call-done = bf16[32,80,2048]{2,1,0:T(8,128)(2,1)} async-done(((bf16[8,80,2048]{2,1,0:T(8,128)(2,1)}), bf16[32,80,2048]{2,1,0:T(8,128)(2,1)}) %all-gather.3.cloned.1.call-update) | async-done | bytes 10485776 | tf_op jit(solution)/shard_map/all_gather | solution.py:80
  155.8 9.1 %fusion = f32[2,32,40,256]{3,2,1,0:T(8,128)} fusion(bf16[32,2,40,2048]{3,2,1,0:T(8,128)(2,1)} %bitcast.93, bf16[2,2048,256]{2,1,0:T(8,128)(2,1)} %param.23), kind=kOutput, calls=%fused_computation.4 | convolution fusion | flops 2684354560 | bytes 15204352 | tf_op jit(solution)/shard_map/nxcd,xdf->nxcf/dot_general | solution.py:96
  164.9 0.0 copy-done
  164.9 16.4 %convert_bitcast_fusion = bf16[32,2,40,2048]{3,2,0,1:T(8,128)(2,1)} fusion(bf16[2,256,2048]{2,1,0:T(8,128)(2,1)S(1)} %copy-done, f32[2,32,40,256]{3,2,1,0:T(8,128)} %fusion, bf16[2,2048,256]{2,1,0:T(8,128)(2,1)} %param.22, bf16[32,2,40,2048]{3,2,1,0:T(8,128)(2,1)} %bitcast.94), kind=kOutput, calls=%fused_computation.3 | convolution fusion | flops 5377884160 | bytes 27787264 | tf_op jit(solution)/shard_map/nxcf,xfd->nxcd/dot_general | solution.py:98
  181.3 10.2 %copy.34 = bf16[32,2,40,2048]{3,2,1,0:T(8,128)(2,1)} copy(bf16[32,2,40,2048]{3,2,0,1:T(8,128)(2,1)} %convert_bitcast_fusion) | data formatting | bytes 20971520 | tf_op jit(solution)/shard_map/convert_element_type | solution.py:100
  191.5 0.0 copy-start.4
  191.5 0.0 reduce-scatter.5.cloned.1.call-update
  191.5 0.0 reduce-scatter.3.cloned.1.call-start
  191.6 0.9 copy-done.4
  192.5 3.4 collective-permute-start
  195.9 1.3 collective-permute-done
  197.2 0.1 fusion.38
  197.3 0.7 fusion.27
  198.0 0.0 copy-start.3
  198.0 0.0 copy-start.5
  198.0 0.0 copy-start.8
  198.1 0.1 broadcast_add_fusion
  198.1 0.2 copy.27
  198.4 0.8 copy-done.3
  199.2 0.0 copy-done.5
  199.2 0.0 copy-done.8
  199.2 2.4 convolution_convert_fusion
  201.6 0.0 reduce-scatter.3.cloned.1.call-update
  201.6 74.5 %reduce-scatter.5.cloned.1.call-done = bf16[640,2048]{1,0:T(8,128)(2,1)} async-done(((bf16[2560,2048]{1,0:T(8,128)(2,1)}), bf16[640,2048]{1,0:T(8,128)(2,1)}) %reduce-scatter.5.cloned.1.call-update) | async-done | bytes 2621456 | tf_op jit(solution)/shard_map/reduce_scatter | solution.py:99
  276.1 0.0 copy-start.6
  276.1 5.6 %all-to-all-start.1 = ((bf16[8,80,2048]{2,1,0:T(8,128)(2,1)}), bf16[8,80,2048]{2,1,0:T(8,128)(2,1)S(1)}, u32[]{:S(2)}, u32[]{:S(2)}) async-start(bf16[8,80,2048]{2,1,0:T(8,128)(2,1)} %bitcast.87), calls=%async_computation.3 | async-start | bytes 5242880 | tf_op jit(solution)/shard_map/all_to_all | solution.py:107
  281.7 0.7 constant_dynamic-slice_fusion
  282.4 0.1 copy.35
  282.6 27.2 %reduce-scatter.3.cloned.1.call-done = bf16[128,2048]{1,0:T(8,128)(2,1)} async-done(((bf16[512,2048]{1,0:T(8,128)(2,1)}), bf16[128,2048]{1,0:T(8,128)(2,1)}) %reduce-scatter.3.cloned.1.call-update) | async-done | bytes 524304 | tf_op jit(solution)/shard_map/reduce_scatter | solution.py:83
  309.8 1.2 fusion.24
  311.0 0.0 copy-done.6
  311.1 2.0 fusion.26
  313.1 28.0 %all-to-all-done.1 = bf16[8,80,2048]{2,1,0:T(8,128)(2,1)S(1)} async-done(((bf16[8,80,2048]{2,1,0:T(8,128)(2,1)}), bf16[8,80,2048]{2,1,0:T(8,128)(2,1)S(1)}, u32[]{:S(2)}, u32[]{:S(2)}) %all-to-all-start.1) | async-done | bytes 2621472 | tf_op jit(solution)/shard_map/all_to_all | solution.py:107
  341.0 3.3 gather_fusion.1
  344.4 5.4 %reshape.116 = f32[256,2,2048]{2,1,0:T(2,128)} reshape(bf16[512,2048]{1,0:T(8,128)(2,1)} %gather_fusion.1) | data formatting | bytes 6291456 | tf_op jit(solution)/shard_map/convert_element_type | solution.py:112
  349.8 0.0 copy-start.7
  349.8 0.0 copy-start.1
  349.8 9.0 %multiply_reduce_fusion = f32[256,2048]{1,0:T(8,128)S(1)} fusion(f32[256,2,2048]{2,1,0:T(2,128)} %reshape.116, f32[256,2]{1,0:T(8,128)S(1)} %copy.35), kind=kLoop, calls=%fused_computation.8 | loop fusion | flops 1572864 | bytes 6293504 | tf_op jit(solution)/shard_map/reduce_sum | solution.py:112
  358.8 0.2 multiply_reduce_fusion.1
  359.1 0.0 copy-done.7
  359.1 1.2 multiply_convert_fusion
  360.3 0.0 copy-done.1
  (17 shorter events, 0.2 us)
Async XLA Ops:
  7.2 157.8 %copy-start = (bf16[2,256,2048]{2,1,0:T(8,128)(2,1)S(1)}, bf16[2,256,2048]{2,1,0:T(8,128)(2,1)}, u32[]{:S(2)}) copy-start(bf16[2,256,2048]{2,1,0:T(8,128)(2,1)} %param.24) | copy-start | bytes 6291460
  7.2 7.2 %copy-start.2 = (bf16[256,2048]{1,0:T(8,128)(2,1)S(1)}, bf16[256,2048]{1,0:T(8,128)(2,1)}, u32[]{:S(2)}) copy-start(bf16[256,2048]{1,0:T(8,128)(2,1)} %param.18) | copy-start | bytes 3145732
  7.2 148.6 %all-gather.3.cloned.1.call-start = ((), (), s32[]{:S(2)}) async-start(), calls=%async_computation.6 | async-start | bytes 13107200 | tf_op jit(solution)/shard_map/all_gather | solution.py:80
  86.5 189.6 %reduce-scatter.5.cloned.1.call-start = ((), (), s32[]{:S(2)}) async-start(), calls=%async_computation.5 | async-start | bytes 13107200 | tf_op jit(solution)/shard_map/reduce_scatter | solution.py:99
  191.5 0.9 copy-start.4
  191.5 118.3 %reduce-scatter.3.cloned.1.call-start = ((), (), s32[]{:S(2)}) async-start(), calls=%async_computation.4 | async-start | bytes 2621440 | tf_op jit(solution)/shard_map/reduce_scatter | solution.py:83
  192.5 4.7 %collective-permute-start = (bf16[16,256]{1,0:T(8,128)(2,1)S(1)}, bf16[16,256]{1,0:T(8,128)(2,1)S(1)}, u32[]{:S(2)}, u32[]{:S(2)}) collective-permute-start(bf16[16,256]{1,0:T(8,128)(2,1)S(1)} %slice.25), channel_id=1, source_target_pairs={{0,4},{4,8},{8,12},{12,16},{16,20},{20,24},{24,28},{1,5},{5,9},{9,... | collective-permute-start | bytes 24584 | tf_op jit(solution)/shard_map/ppermute | solution.py:12
  198.0 1.2 copy-start.3
  198.0 1.2 copy-start.5
  198.0 1.2 copy-start.8
  276.1 35.0 %copy-start.6 = (f32[2048]{0:T(1024)S(1)}, f32[2048]{0:T(1024)}, u32[]{:S(2)}) copy-start(f32[2048]{0:T(1024)} %param.17) | copy-start | bytes 24580
  276.1 64.9 %all-to-all-start.1 = ((bf16[8,80,2048]{2,1,0:T(8,128)(2,1)}), bf16[8,80,2048]{2,1,0:T(8,128)(2,1)S(1)}, u32[]{:S(2)}, u32[]{:S(2)}) async-start(bf16[8,80,2048]{2,1,0:T(8,128)(2,1)} %bitcast.87), calls=%async_computation.3 | async-start | bytes 5242880 | tf_op jit(solution)/shard_map/all_to_all | solution.py:107
  349.8 9.3 %copy-start.7 = (f32[2048]{0:T(1024)S(1)}, f32[2048]{0:T(1024)}, u32[]{:S(2)}) copy-start(f32[2048]{0:T(1024)} %param.25) | copy-start | bytes 24580
  349.8 10.5 %copy-start.1 = (bf16[2,256,2048]{2,1,0:T(8,128)(2,1)S(1)}, bf16[2,256,2048]{2,1,0:T(8,128)(2,1)}, u32[]{:S(2)}) copy-start(bf16[2,256,2048]{2,1,0:T(8,128)(2,1)} %param.24) | copy-start | bytes 6291460
Sparse Core Ops, SparseCore 0:
  86.6 69.1 all-gather.2
  191.7 84.3 reduce-scatter.4
  278.6 31.1 reduce-scatter.2
where the time goes:
time: 367 us
  waiting for transfers between devices  200 us (54%)
  blocking collectives  66.9 us (18%)
  local copies, waits for them, and re-layouts  29.3 us (8%)
  matrix products  27.9 us (8%)
  other arithmetic  19.3 us (5%)
  between operations  14 us (4%)
  starting transfers between devices  9.31 us (3%)
    reduce_scatter x1, waiting for transfers between devices, on_device(): lax.psum_scatter(down_act.reshape(per_quarter * lax.axis_size('tp'), mode...  74.5 us
    all_gather x1, waiting for transfers between devices, on_device(): received = lax.all_gather(arrived[None], 'tp', axis=0, tiled=True)  69.1 us
    all_to_all x1, blocking collectives, on_device(): lax.all_to_all(outgoing, 'ep', split_axis=0, concat_axis=0, tiled=True)  66.9 us
    all_to_all x1, waiting for transfers between devices, on_device(): lax.all_to_all(expert_back, 'ep', split_axis=0, concat_axis=0, tiled=True)  28 us
    reduce_scatter x1, waiting for transfers between devices, on_device(): lax.psum_scatter(jnp.dot(grouped, out_weight, preferred_element_type=jnp....  27.2 us
    dot_general x1, matrix products, on_device(): jnp.einsum('nxcf,xfd->nxcd', hidden, down_weight, preferred_element_type=...  16.4 us
    convert_element_type x1, local copies, waits for them, and re-layouts, on_device(): down_act.reshape(per_quarter * lax.axis_size('tp'), model_width)  10.2 us
    dot_general x1, matrix products, on_device(): jnp.einsum('nxcd,xdf->nxcf', piece_rows, up_weight, preferred_element_typ...  9.11 us
  transfers between devices with their start and end apart: 5, of which 5 were waited for; matrix products, arithmetic and copies ran while one was open for 2% of the time, Pallas kernels for 0%

commit v1 on v0

v1 whole, which is shorter than its diff:
```python
import functools

import jax
import jax.numpy as jnp
from jax import lax
from jax.experimental import pallas as pl
from jax.experimental.pallas import tpu as pltpu
from jax.sharding import PartitionSpec as P

NORM_EPS = 1e-06


def passed_along(value, axis, steps):
    count = lax.axis_size(axis)
    initial, last = (max(0, -steps), min(count, count - steps))
    return lax.ppermute(value, axis, [(source, source + steps) for source in range(initial, last)])


def rms_scale(values, gain_vec):
    mean_sq = jnp.mean(values * values, axis=-1, keepdims=True)
    return values * lax.rsqrt(mean_sq + NORM_EPS) * gain_vec


def slot_numbers(route_block, experts, capacity, exp_dev, block_rows):
    flat_routes = route_block.reshape(-1)
    one_hot = (flat_routes[:, None] == jnp.arange(experts, dtype=jnp.int32)[None, :]).astype(
        jnp.int32
    )
    slot_rank = jnp.sum((jnp.cumsum(one_hot, axis=0) - one_hot) * one_hot, axis=1)
    owner = flat_routes // exp_dev
    local = flat_routes - owner * exp_dev
    return owner * block_rows + local * capacity + slot_rank


def fill_table(slot_ids, payload, empty_value, slots_total):
    return jnp.full((slots_total,), empty_value, payload.dtype).at[slot_ids].set(payload)


MESH = pl.DeviceIdType.MESH


def exchange_kernel(
    capacity,
    outgoing,
    mix_part,
    gate_hbm,
    up_hbm,
    down_hbm,
    returned,
    projected,
    arrived,
    part,
    core_in,
    chip_sum,
    cross_in,
    final,
    gate,
    up,
    down,
    mix_held,
    mix_core,
    mix_sum,
    mix_cross,
    local_sem,
    dis_send,
    dis_recv,
    y1_send,
    y1_recv,
    c1_send,
    c1_recv,
    c2_send,
    c2_recv,
    y2_send,
    y2_recv,
    ret_send,
    ret_recv,
    m1_send,
    m1_recv,
    m2_send,
    m2_recv,
):
    ep_size, tp_size, rows, width = arrived.shape
    exp_dev, _, ff_dev = gate.shape
    highs = tp_size // 2
    ep = lax.axis_index("ep")
    tp = lax.axis_index("tp")
    hi, lo = tp // 2, tp % 2
    other = 1 - lo

    def remote(src, dst, send, recv, to_ep, to_tp):
        return pltpu.make_async_remote_copy(
            src_ref=src,
            dst_ref=dst,
            send_sem=send,
            recv_sem=recv,
            device_id=(to_ep, to_tp),
            device_id_type=MESH,
        )

    def peer_high(k):
        return lax.rem(hi + k, highs)

    def offset_of(i):
        return jnp.where(i < 2, i, ep_size + 1 - i)

    def partner_ep(d):
        low = d
        mine = ep
        value = ep * 0
        bit = 1
        while bit < ep_size:
            a = (mine // bit) % 2
            b = (low // bit) % 2
            value = value + bit * ((a + b) % 2)
            bit *= 2
        return value

    def dispatch(d):
        peer = partner_ep(d)
        return remote(
            outgoing.at[peer], arrived.at[d, tp], dis_send.at[d], dis_recv.at[d], peer, tp
        )

    def gather_cross(d, k):
        high = peer_high(k)
        return remote(
            arrived.at[d, tp],
            arrived.at[d, tp],
            y1_send.at[d, k],
            y1_recv.at[d, highs - k],
            ep,
            high * 2 + lo,
        )

    def gather_cross_in(d, k):
        high = peer_high(k)
        return remote(
            arrived.at[d, high * 2 + lo],
            arrived.at[d, high * 2 + lo],
            y1_send.at[d, k],
            y1_recv.at[d, k],
            ep,
            high * 2 + lo,
        )

    def gather_core(d, high):
        slot = arrived.at[d, high * 2 + lo]
        return remote(slot, slot, c1_send.at[d, high], c1_recv.at[d, high], ep, hi * 2 + other)

    def gather_core_in(d, high):
        slot = arrived.at[d, high * 2 + other]
        return remote(slot, slot, c1_send.at[d, high], c1_recv.at[d, high], ep, hi * 2 + other)

    def reduce_core(d, high):
        return remote(
            part.at[high * 2 + other],
            core_in.at[d, high],
            c2_send.at[d, high],
            c2_recv.at[d, high],
            ep,
            hi * 2 + other,
        )

    def reduce_cross(d, k):
        high = peer_high(k)
        return remote(
            chip_sum.at[high],
            cross_in.at[d, highs - k - 1],
            y2_send.at[d, k],
            y2_recv.at[d, highs - k],
            ep,
            high * 2 + lo,
        )

    def reduce_cross_in(d, k):
        high = peer_high(k)
        return remote(
            chip_sum.at[high],
            cross_in.at[d, k - 1],
            y2_send.at[d, k],
            y2_recv.at[d, k],
            ep,
            high * 2 + lo,
        )

    def give_back(d):
        peer = partner_ep(d)
        return remote(final.at[d], returned.at[ep], ret_send.at[d], ret_recv.at[d], peer, tp)

    def give_back_in(d):
        peer = partner_ep(d)
        return remote(final.at[d], returned.at[peer], ret_send.at[d], ret_recv.at[d], peer, tp)

    def mix_core_copy(high):
        return remote(
            mix_held.at[high * 2 + other],
            mix_core.at[high],
            m1_send.at[high],
            m1_recv.at[high],
            ep,
            hi * 2 + other,
        )

    def mix_cross_copy(k):
        high = peer_high(k)
        return remote(
            mix_sum.at[high],
            mix_cross.at[highs - k - 1],
            m2_send.at[k],
            m2_recv.at[highs - k],
            ep,
            high * 2 + lo,
        )

    def mix_cross_in(k):
        high = peer_high(k)
        return remote(
            mix_sum.at[high],
            mix_cross.at[k - 1],
            m2_send.at[k],
            m2_recv.at[k],
            ep,
            high * 2 + lo,
        )

    own_rows = pltpu.make_async_copy(outgoing.at[ep], arrived.at[0, tp], local_sem.at[0])
    own_mix = pltpu.make_async_copy(mix_part, mix_held, local_sem.at[1])
    weight_copies = [
        pltpu.make_async_copy(gate_hbm, gate, local_sem.at[2]),
        pltpu.make_async_copy(up_hbm, up, local_sem.at[3]),
        pltpu.make_async_copy(down_hbm, down, local_sem.at[4]),
    ]
    own_rows.start()
    own_mix.start()
    for copy in weight_copies:
        copy.start()

    barrier = pltpu.get_barrier_semaphore()

    def greet(d, carry):
        pl.semaphore_signal(barrier, inc=1, device_id=(partner_ep(d), tp), device_id_type=MESH)
        return carry

    lax.fori_loop(1, ep_size, greet, 0)
    for k in range(1, highs):
        pl.semaphore_signal(
            barrier, inc=1, device_id=(ep, peer_high(k) * 2 + lo), device_id_type=MESH
        )
    pl.semaphore_signal(barrier, inc=1, device_id=(ep, hi * 2 + other), device_id_type=MESH)
    pl.semaphore_wait(barrier, ep_size - 1 + highs)

    def send_out(i, carry):
        dispatch(offset_of(i)).start()
        return carry

    lax.fori_loop(1, ep_size, send_out, 0)

    def stage_a(d):
        for k in range(1, highs):
            gather_cross(d, k).start()
        gather_core(d, hi).start()

    own_rows.wait()
    stage_a(0)

    own_mix.wait()
    for high in range(highs):
        mix_core_copy(high).start()
    for high in range(highs):
        mix_core_copy(high).wait_recv()
    for high in range(highs):
        mix_sum[high] = (
            mix_held[high * 2 + lo].astype(jnp.float32) + mix_core[high].astype(jnp.float32)
        ).astype(jnp.bfloat16)
    for k in range(1, highs):
        mix_cross_copy(k).start()
    for copy in weight_copies:
        copy.wait()

    row_expert = (
        lax.rem(lax.broadcasted_iota(jnp.int32, (tp_size * rows, 1), 0), rows) // capacity
    )
    column_step = min(width, 512)

    def step(i, carry):
        @pl.when(i + 1 < ep_size)
        def _():
            d = offset_of(i + 1)
            dispatch(d).wait_recv()
            stage_a(d)

        @pl.when(i < ep_size)
        def _():
            d = offset_of(i)
            for k in range(1, highs):
                gather_cross_in(d, k).wait_recv()
                gather_core(d, peer_high(k)).start()

        @pl.when(i >= 2)
        def _():
            d = offset_of(i - 2)
            total = chip_sum[hi].astype(jnp.float32)
            for k in range(1, highs):
                reduce_cross(d, k).wait_send()
                reduce_cross_in(d, k).wait_recv()
                total = total + cross_in[d, k - 1].astype(jnp.float32)
            final[d] = total.astype(jnp.bfloat16)

            @pl.when(i == 2)
            def _():
                pltpu.make_async_copy(final.at[0], returned.at[ep], local_sem.at[0]).start()

            @pl.when(i > 2)
            def _():
                give_back(d).start()

        @pl.when((i >= 1) & (i <= ep_size))
        def _():
            d = offset_of(i - 1)
            for high in range(highs):
                reduce_core(d, high).wait_recv()
                reduce_core(d, high).wait_send()
                chip_sum[high] = (
                    part[high * 2 + lo].astype(jnp.float32) + core_in[d, high].astype(jnp.float32)
                ).astype(jnp.bfloat16)
            for k in range(1, highs):
                reduce_cross(d, k).start()

        @pl.when(i < ep_size)
        def _():
            d = offset_of(i)
            for high in range(highs):
                gather_core_in(d, high).wait_recv()
            hidden = []
            for e in range(exp_dev):
                block = arrived[d].reshape(tp_size * rows, width)
                gate_act = jnp.dot(block, gate[e], preferred_element_type=jnp.float32)
                up_act = jnp.dot(block, up[e], preferred_element_type=jnp.float32)
                act = gate_act / (1.0 + jnp.exp(-gate_act)) * up_act
                hidden.append(jnp.where(row_expert == e, act, 0.0).astype(jnp.bfloat16))
            joined = jnp.concatenate(hidden, axis=1)
            for start in range(0, width, column_step):
                columns = slice(start, start + column_step)
                out = jnp.dot(
                    joined,
                    down[:, :, columns].reshape(exp_dev * ff_dev, column_step),
                    preferred_element_type=jnp.float32,
                )
                part[:, :, columns] = out.astype(jnp.bfloat16).reshape(tp_size, rows, column_step)
            for high in range(highs):
                reduce_core(d, high).start()

        return carry

    lax.fori_loop(0, ep_size + 2, step, 0)

    total = mix_sum[hi].astype(jnp.float32)
    for k in range(1, highs):
        mix_cross_in(k).wait_recv()
        total = total + mix_cross[k - 1].astype(jnp.float32)
    projected[...] = total
    for k in range(1, highs):
        mix_cross_copy(k).wait_send()
    for high in range(highs):
        mix_core_copy(high).wait_send()

    def drain_all(d, carry):
        for k in range(1, highs):
            gather_cross(d, k).wait_send()
        for high in range(highs):
            gather_core(d, high).wait_send()
        return carry

    lax.fori_loop(0, ep_size, drain_all, 0)

    def drain(i, carry):
        d = offset_of(i)
        dispatch(d).wait_send()
        give_back(d).wait_send()
        give_back_in(d).wait_recv()
        return carry

    lax.fori_loop(1, ep_size, drain, 0)
    pltpu.make_async_copy(final.at[0], returned.at[ep], local_sem.at[0]).wait()


def exchange(outgoing, mix_part, gate_weight, up_weight, down_weight, capacity):
    ep_size, rows, width = outgoing.shape
    tp_size, mix_rows, _ = mix_part.shape
    highs = tp_size // 2
    bf16 = jnp.bfloat16
    any_spec = pl.BlockSpec(memory_space=pl.ANY)
    dma = pltpu.SemaphoreType.DMA
    pair = (ep_size, highs)
    flops = 6 * gate_weight.size * ep_size * tp_size * rows
    return pl.pallas_call(
        functools.partial(exchange_kernel, capacity),
        out_shape=(
            jax.ShapeDtypeStruct(outgoing.shape, bf16),
            jax.ShapeDtypeStruct((mix_rows, width), jnp.float32),
        ),
        in_specs=[any_spec] * 5,
        out_specs=(any_spec, pl.BlockSpec(memory_space=pltpu.VMEM)),
        scratch_shapes=[
            pltpu.VMEM((ep_size, tp_size, rows, width), bf16),
            pltpu.VMEM((tp_size, rows, width), bf16),
            pltpu.VMEM((ep_size, highs, rows, width), bf16),
            pltpu.VMEM((highs, rows, width), bf16),
            pltpu.VMEM((ep_size, highs - 1, rows, width), bf16),
            pltpu.VMEM((ep_size, rows, width), bf16),
            pltpu.VMEM(gate_weight.shape, bf16),
            pltpu.VMEM(up_weight.shape, bf16),
            pltpu.VMEM(down_weight.shape, bf16),
            pltpu.VMEM(mix_part.shape, bf16),
            pltpu.VMEM((highs, mix_rows, width), bf16),
            pltpu.VMEM((highs, mix_rows, width), bf16),
            pltpu.VMEM((highs - 1, mix_rows, width), bf16),
            dma((5,)),
            dma((ep_size,)),
            dma((ep_size,)),
            dma(pair),
            dma(pair),
            dma(pair),
            dma(pair),
            dma(pair),
            dma(pair),
            dma(pair),
            dma(pair),
            dma((ep_size,)),
            dma((ep_size,)),
            dma((highs,)),
            dma((highs,)),
            dma((highs,)),
            dma((highs,)),
        ],
        compiler_params=pltpu.CompilerParams(
            collective_id=0, has_side_effects=True, vmem_limit_bytes=60 * 1024 * 1024
        ),
        cost_estimate=pl.CostEstimate(
            flops=flops, bytes_accessed=4 * outgoing.size, transcendentals=0
        ),
    )(outgoing, mix_part, gate_weight, up_weight, down_weight)


def on_device(
    pool_input,
    group_weight,
    pool_scale,
    out_weight,
    mix_gain,
    expert_input,
    routes,
    route_weights,
    moe_in_gain,
    gate_weight,
    up_weight,
    down_weight,
    moe_out_gain,
):
    tp_size = lax.axis_size("tp")
    ep_size = lax.axis_size("ep")
    tp_index = lax.axis_index("tp")
    rows_a = pool_input.shape[0]
    model_width = out_weight.shape[1]
    history_rows = 2**tp_size
    window = jnp.left_shift(jnp.int32(2), tp_index)
    history = passed_along(pool_input[rows_a - history_rows :], "ep", 1)
    extended = jnp.concatenate([history, pool_input], axis=0).astype(jnp.float32)
    running = jnp.cumsum(extended, axis=0)
    lagged = lax.dynamic_slice_in_dim(running, history_rows - window, rows_a, 0)
    current = running[history_rows:]
    position = lax.axis_index("ep") * rows_a + jnp.arange(rows_a, dtype=jnp.int32)
    divisor = jnp.minimum(position + 1, window).astype(jnp.float32)[:, None]
    pooled = ((current - lagged) / divisor - extended[history_rows:]).astype(jnp.bfloat16)
    grouped = (
        jnp.dot(pooled, group_weight[0], preferred_element_type=jnp.float32) * pool_scale
    ).astype(jnp.bfloat16)
    exp_dev = gate_weight.shape[0]
    experts = exp_dev * ep_size
    tok_dev = expert_input.shape[0]
    top_count = routes.shape[1]
    capacity = max(2, 5 * tok_dev * top_count // (4 * experts))
    block_rows = -(-exp_dev * capacity // 16) * 16
    slots_total = ep_size * block_rows
    normed = rms_scale(expert_input.astype(jnp.float32), moe_in_gain).astype(jnp.bfloat16)
    own_routes = lax.dynamic_slice_in_dim(routes, tp_index * tok_dev, tok_dev, 0)
    own_slots = slot_numbers(own_routes, experts, capacity, exp_dev, block_rows)
    pair_token = jnp.arange(tok_dev * top_count, dtype=jnp.int32) // top_count
    token_table = fill_table(own_slots, pair_token, tok_dev, slots_total)
    padded_rows = jnp.concatenate([normed, jnp.zeros((1, model_width), jnp.bfloat16)], axis=0)
    outgoing = padded_rows[token_table].reshape(ep_size, block_rows, model_width)
    mix_part = (
        jnp.dot(grouped, out_weight, preferred_element_type=jnp.float32)
        .astype(jnp.bfloat16)
        .reshape(tp_size, rows_a // tp_size, model_width)
    )
    returned, projected = exchange(
        outgoing, mix_part, gate_weight, up_weight, down_weight, capacity
    )
    mixer_out = rms_scale(projected, mix_gain).astype(jnp.bfloat16)
    back = returned.reshape(slots_total, model_width)
    slot_pairs = own_slots.reshape(tok_dev, top_count)
    own_weights = lax.dynamic_slice_in_dim(route_weights, tp_index * tok_dev, tok_dev, 0)
    combined = jnp.zeros((tok_dev, model_width), jnp.float32)
    for k in range(top_count):
        combined = combined + back[slot_pairs[:, k]].astype(jnp.float32) * own_weights[:, k : k + 1]
    moe_out = rms_scale(combined, moe_out_gain).astype(jnp.bfloat16)
    return (mixer_out, moe_out)


def solution(mesh):
    in_specs = (
        P("ep", "tp"),
        P("tp", None, None),
        P("tp"),
        P("tp", None),
        P(),
        P(("ep", "tp"), None),
        P("ep", None),
        P("ep", None),
        P(),
        P("ep", None, "tp"),
        P("ep", None, "tp"),
        P("ep", "tp", None),
        P(),
    )
    out_specs = (P(("ep", "tp"), None), P(("ep", "tp"), None))
    return jax.shard_map(
        on_device, mesh=mesh, in_specs=in_specs, out_specs=out_specs, check_vma=False
    )
```

time: 367 us -> 193 us (0.53)
  waiting for transfers between devices: 200 us -> 0.01 us
  Pallas kernels: 0 us -> 157 us
  blocking collectives: 66.9 us -> 0 us
  matrix products: 27.9 us -> 2.28 us
  between operations: 14 us -> 0.94 us
  other arithmetic: 19.3 us -> 6.37 us
  local copies, waits for them, and re-layouts: 29.3 us -> 20.4 us
  starting transfers between devices: 9.31 us -> 4.86 us
    pallas_call x0 -> x1, Pallas kernels: none -> 157 us  [exchange(): pl.pallas_call(functools.partial(exchange_kernel, capacity), out_shape=(j...]
    reduce_scatter x2 -> x0, waiting for transfers between devices: 102 us -> none  [the longest x1 74.5 us: on_device(): lax.psum_scatter(down_act.reshape(per_quarter * lax.axis_size('tp'), mode...]
    all_gather x1 -> x0, waiting for transfers between devices: 69.1 us -> none  [on_device(): received = lax.all_gather(arrived[None], 'tp', axis=0, tiled=True)]
    all_to_all x1 -> x0, blocking collectives: 66.9 us -> none  [on_device(): lax.all_to_all(outgoing, 'ep', split_axis=0, concat_axis=0, tiled=True)]
    all_to_all x1 -> x0, waiting for transfers between devices: 28 us -> none  [on_device(): lax.all_to_all(expert_back, 'ep', split_axis=0, concat_axis=0, tiled=True)]
    dot_general x2 -> x0, matrix products: 25.5 us -> none  [the longest x1 16.4 us: on_device(): jnp.einsum('nxcf,xfd->nxcd', hidden, down_weight, preferred_element_type=...]
    convert_element_type x2 -> x0, local copies, waits for them, and re-layouts: 15.6 us -> none  [the longest x1 10.2 us: on_device(): down_act.reshape(per_quarter * lax.axis_size('tp'), model_width)]
    reduce_sum x1 -> x0, other arithmetic: 9.02 us -> none  [on_device(): jnp.sum(picked.astype(jnp.float32) * own_weights[:, :, None], axis=1)]
  transfers between devices with their start and end apart: 5 -> 1, of which waited for: 5 -> 0; matrix products, arithmetic and copies ran while one was open for 2% -> 6% of each run, Pallas kernels for 0% -> 0%
where the time goes in v1:
time: 193 us; the launch traced here: 192 us
  Pallas kernels  157 us (81%)
  local copies, waits for them, and re-layouts  20.4 us (11%)
  other arithmetic  6.37 us (3%)
  starting transfers between devices  4.86 us (3%)
  matrix products  2.28 us (1%)
    pallas_call x1, Pallas kernels, exchange(): pl.pallas_call(functools.partial(exchange_kernel, capacity), out_shape=(j...  157 us
    gather x2, local copies, waits for them, and re-layouts, on_device(): back[slot_pairs[:, k]].astype(jnp.float32) * own_weights[:, k:k + 1]  8.88 us
    ppermute x1, starting transfers between devices, passed_along(): lax.ppermute(value, axis, [(source, source + steps) for source in range(i...  4.86 us
    gather x1, local copies, waits for them, and re-layouts, on_device(): padded_rows[token_table].reshape(ep_size, block_rows, model_width)  4.27 us
  transfers between devices with their start and end apart: 1, of which 0 were waited for; matrix products, arithmetic and copies ran while one was open for 6% of the time, Pallas kernels for 0%

profile of v1, /device:TPU:0, one launch (start us, length us, event | category | flops | bytes accessed | tf_op | source)
XLA Modules:
  0.0 192.2 jit_solution(7797941698603999987)
XLA Ops:
  0.6 0.0 copy-start
  0.6 0.0 copy-start.1
  0.7 0.0 copy-start.5
  0.7 0.8 slice.39
  1.5 4.9 %collective-permute-start = (bf16[16,256]{1,0:T(8,128)(2,1)S(1)}, bf16[16,256]{1,0:T(8,128)(2,1)S(1)}, u32[]{:S(2)}, u32[]{:S(2)}) collective-permute-start(bf16[16,256]{1,0:T(8,128)(2,1)S(1)} %slice.39), channel_id=1, source_target_pairs={{0,4},{4,8},{8,12},{12,16},{16,20},{20,24},{24,28},{1,5},{5,9},{9,... | collective-permute-start | bytes 24584 | tf_op jit(solution)/shard_map/ppermute | solution.py:16
  6.4 0.7 constant_dynamic-slice_fusion.1
  7.1 0.1 copy.24
  7.2 0.1 eq.29
  7.4 0.1 eq.25
  7.5 0.1 reshape.187
  7.7 1.2 reduce-window.14
  8.8 0.2 slice_reduce_fusion
  9.1 0.1 fusion.22
  9.2 0.1 reduce_sum.44
  9.3 0.1 add_add_fusion
  9.4 0.2 fusion.14
  9.7 2.4 %scatter_custom_fusion = s32[640]{0:T(1024)S(1)} fusion(s32[512]{0:T(512)S(1)} %bitcast.53, s32[512]{0:T(512)S(1)} %add_select_fusion.1, s32[]{:T(128)} %constant.64.clone.1), kind=kCustom, calls=%fused_computation.67 | custom fusion | bytes 2564 | tf_op jit(solution)/shard_map/scatter | solution.py:36
  12.2 0.0 copy-done.1
  12.2 0.3 fusion
  12.5 0.0 copy-done.5
  12.5 0.3 fusion.2
  12.8 0.8 constant_dynamic-slice_fusion
  13.7 0.1 concatenate.6
  13.8 0.0 copy-start.3
  13.8 4.3 %gather_fusion = bf16[640,2048]{1,0:T(8,128)(2,1)} fusion(bf16[257,2048]{1,0:T(8,128)(2,1)S(1)} %concatenate.6, s32[1024]{0:T(1024)S(1)} %pad_clamp_fusion.2), kind=kCustom, calls=%fused_computation | custom fusion | bytes 5245440 | tf_op jit(solution)/shard_map/gather | solution.py:491
  18.1 0.0 collective-permute-done
  18.1 0.0 copy-done.3
  18.1 0.1 fusion.19
  18.2 0.7 fusion.4
  18.9 0.0 copy-start.4
  18.9 0.0 copy-start.8
  18.9 0.1 broadcast_add_fusion
  19.0 0.2 copy.23
  19.3 0.0 copy-done
  19.3 0.5 copy-done.4
  19.8 0.0 copy-done.8
  19.8 2.3 %convolution_convert_fusion = bf16[512,2048]{1,0:T(8,128)(2,1)} fusion(bf16[256,2048]{1,0:T(8,128)(2,1)S(1)} %copy-done, f32[528,256]{1,0:T(8,128)S(1)} %get-tuple-element.9, f32[640,256]{1,0:T(8,128)S(1)} %bitcast.43, f32[528,256]{1,0:T(8,128)S(1)} %slice.59, s32[]{:T(128)S(6)} %select_n.51, f32[256]{0:T(256)S(1)} %copy-done.8, ...), kind=kOutput, calls=%fused_computation.4 | convolution fusion | flops 605814784 | bytes 4852740 | tf_op jit(solution)/shard_map/dot_general | solution.py:493
  22.1 157.3 %shard_map.140 = (bf16[8,80,2048]{2,1,0:T(8,128)(2,1)}, f32[128,2048]{1,0:T(8,128)}) custom-call(bf16[8,80,2048]{2,1,0:T(8,128)(2,1)} %bitcast.44, bf16[4,128,2048]{2,1,0:T(8,128)(2,1)} %bitcast.46, bf16[2,2048,256]{2,1,0:T(8,128)(2,1)} %gate_hbm.1, bf16[2,2048,256]{2,1,0:T(8,128)(2,1)} %up_hbm.1, bf16[2,256,2048]{2,1,0:T(8,128)(2,1)} %down_hbm.1), custom_call_target="tpu_custom_call" | custom-call | flops 16106127360 | bytes 5242880 | tf_op jit(solution)/shard_map/pallas_call | solution.py:396
  179.4 4.4 %gather_fusion.1 = bf16[256,2048]{1,0:T(8,128)(2,1)S(1)} fusion(bf16[640,2048]{1,0:T(8,128)(2,1)} %bitcast.40, s32[1024]{0:T(1024)S(1)} %get-tuple-element.13), kind=kCustom, calls=%fused_computation.1 | custom fusion | bytes 2098176 | tf_op jit(solution)/shard_map/gather | solution.py:506
  183.8 4.4 %gather_fusion.2 = bf16[256,2048]{1,0:T(8,128)(2,1)S(1)} fusion(bf16[640,2048]{1,0:T(8,128)(2,1)} %bitcast.41, s32[1024]{0:T(1024)S(1)} %get-tuple-element.12), kind=kCustom, calls=%fused_computation.2 | custom fusion | bytes 2098176 | tf_op jit(solution)/shard_map/gather | solution.py:506
  188.3 0.0 copy-start.2
  188.3 0.0 copy-start.6
  188.3 0.6 multiply_reduce_fusion
  188.9 0.6 copy-done.2
  189.5 0.0 copy-start.7
  189.5 0.2 multiply_reduce_fusion.1
  189.7 0.0 copy-done.6
  189.7 1.6 multiply_convert_fusion
  191.3 0.0 copy-done.7
  191.3 1.0 multiply_convert_fusion.1
  (16 shorter events, 0.2 us)
Async XLA Ops:
  0.6 18.6 %copy-start = (bf16[256,2048]{1,0:T(8,128)(2,1)S(1)}, bf16[256,2048]{1,0:T(8,128)(2,1)}, u32[]{:S(2)}) copy-start(bf16[256,2048]{1,0:T(8,128)(2,1)} %param.16) | copy-start | bytes 3145732
  0.6 11.5 %copy-start.1 = (bf16[256,2048]{1,0:T(8,128)(2,1)S(1)}, bf16[256,2048]{1,0:T(8,128)(2,1)}, u32[]{:S(2)}) copy-start(bf16[256,2048]{1,0:T(8,128)(2,1)} %param.18) | copy-start | bytes 3145732
  0.7 11.8 %copy-start.5 = (f32[2048]{0:T(1024)S(1)}, f32[2048]{0:T(1024)}, u32[]{:S(2)}) copy-start(f32[2048]{0:T(1024)} %param.21) | copy-start | bytes 24580
  1.5 16.6 %collective-permute-start = (bf16[16,256]{1,0:T(8,128)(2,1)S(1)}, bf16[16,256]{1,0:T(8,128)(2,1)S(1)}, u32[]{:S(2)}, u32[]{:S(2)}) collective-permute-start(bf16[16,256]{1,0:T(8,128)(2,1)S(1)} %slice.39), channel_id=1, source_target_pairs={{0,4},{4,8},{8,12},{12,16},{16,20},{20,24},{24,28},{1,5},{5,9},{9,... | collective-permute-start | bytes 24584 | tf_op jit(solution)/shard_map/ppermute | solution.py:16
  13.8 4.3 %copy-start.3 = (bf16[512,256]{1,0:T(8,128)(2,1)S(1)}, bf16[512,256]{1,0:T(8,128)(2,1)}, u32[]{:S(2)}) copy-start(bf16[512,256]{1,0:T(8,128)(2,1)} %param.13) | copy-start | bytes 786436
  18.9 0.9 copy-start.4
  18.9 0.9 copy-start.8
  188.3 1.2 copy-start.2
  188.3 1.4 copy-start.6
  189.5 1.7 copy-start.7

commit v2 on v1

--- a/solution.py
+++ b/solution.py
@@ -30,10 +30,6 @@
     owner = flat_routes // exp_dev
     local = flat_routes - owner * exp_dev
     return owner * block_rows + local * capacity + slot_rank
-
-
-def fill_table(slot_ids, payload, empty_value, slots_total):
-    return jnp.full((slots_total,), empty_value, payload.dtype).at[slot_ids].set(payload)
 
 
 MESH = pl.DeviceIdType.MESH
@@ -101,7 +97,8 @@
         return lax.rem(hi + k, highs)
 
     def offset_of(i):
-        return jnp.where(i < 2, i, ep_size + 1 - i)
+        far = jnp.where(i < 2, 2 * i + 1, ep_size + 1 - i)
+        return jnp.where(i < ep_size - 2, far, 2 * (ep_size - 1 - i))
 
     def partner_ep(d):
         low = d
@@ -253,7 +250,7 @@
         dispatch(offset_of(i)).start()
         return carry
 
-    lax.fori_loop(1, ep_size, send_out, 0)
+    lax.fori_loop(0, ep_size - 1, send_out, 0)
 
     def stage_a(d):
         for k in range(1, highs):
@@ -274,6 +271,9 @@
         ).astype(jnp.bfloat16)
     for k in range(1, highs):
         mix_cross_copy(k).start()
+    first = offset_of(ep * 0)
+    dispatch(first).wait_recv()
+    stage_a(first)
     for copy in weight_copies:
         copy.wait()
 
@@ -283,7 +283,7 @@
     column_step = min(width, 512)
 
     def step(i, carry):
-        @pl.when(i + 1 < ep_size)
+        @pl.when(i + 1 < ep_size - 1)
         def _():
             d = offset_of(i + 1)
             dispatch(d).wait_recv()
@@ -306,11 +306,11 @@
                 total = total + cross_in[d, k - 1].astype(jnp.float32)
             final[d] = total.astype(jnp.bfloat16)
 
-            @pl.when(i == 2)
+            @pl.when(i == ep_size + 1)
             def _():
                 pltpu.make_async_copy(final.at[0], returned.at[ep], local_sem.at[0]).start()
 
-            @pl.when(i > 2)
+            @pl.when(i <= ep_size)
             def _():
                 give_back(d).start()
 
@@ -380,7 +380,7 @@
         give_back_in(d).wait_recv()
         return carry
 
-    lax.fori_loop(1, ep_size, drain, 0)
+    lax.fori_loop(0, ep_size - 1, drain, 0)
     pltpu.make_async_copy(final.at[0], returned.at[ep], local_sem.at[0]).wait()
 
 
@@ -485,10 +485,16 @@
     normed = rms_scale(expert_input.astype(jnp.float32), moe_in_gain).astype(jnp.bfloat16)
     own_routes = lax.dynamic_slice_in_dim(routes, tp_index * tok_dev, tok_dev, 0)
     own_slots = slot_numbers(own_routes, experts, capacity, exp_dev, block_rows)
-    pair_token = jnp.arange(tok_dev * top_count, dtype=jnp.int32) // top_count
-    token_table = fill_table(own_slots, pair_token, tok_dev, slots_total)
-    padded_rows = jnp.concatenate([normed, jnp.zeros((1, model_width), jnp.bfloat16)], axis=0)
-    outgoing = padded_rows[token_table].reshape(ep_size, block_rows, model_width)
+    slot_pairs = own_slots.reshape(tok_dev, top_count)
+    slot_range = jnp.arange(slots_total, dtype=jnp.int32)
+    chosen = slot_pairs[:, 0][None, :] == slot_range[:, None]
+    for k in range(1, top_count):
+        chosen = chosen | (slot_pairs[:, k][None, :] == slot_range[:, None])
+    outgoing = (
+        jnp.dot(chosen.astype(jnp.bfloat16), normed, preferred_element_type=jnp.float32)
+        .astype(jnp.bfloat16)
+        .reshape(ep_size, block_rows, model_width)
+    )
     mix_part = (
         jnp.dot(grouped, out_weight, preferred_element_type=jnp.float32)
         .astype(jnp.bfloat16)
@@ -499,11 +505,12 @@
     )
     mixer_out = rms_scale(projected, mix_gain).astype(jnp.bfloat16)
     back = returned.reshape(slots_total, model_width)
-    slot_pairs = own_slots.reshape(tok_dev, top_count)
     own_weights = lax.dynamic_slice_in_dim(route_weights, tp_index * tok_dev, tok_dev, 0)
     combined = jnp.zeros((tok_dev, model_width), jnp.float32)
     for k in range(top_count):
-        combined = combined + back[slot_pairs[:, k]].astype(jnp.float32) * own_weights[:, k : k + 1]
+        place = (slot_pairs[:, k : k + 1] == slot_range[None, :]).astype(jnp.bfloat16)
+        picked = jnp.dot(place, back, preferred_element_type=jnp.float32)
+        combined = combined + picked * own_weights[:, k : k + 1]
     moe_out = rms_scale(combined, moe_out_gain).astype(jnp.bfloat16)
     return (mixer_out, moe_out)
 

time: 193 us -> 172 us (0.89)
  local copies, waits for them, and re-layouts: 20.4 us -> 4.23 us
  Pallas kernels: 157 us -> 148 us
  matrix products: 2.28 us -> 8.92 us
    gather x3 -> x0, local copies, waits for them, and re-layouts: 13.1 us -> none  [the longest x2 8.88 us: on_device(): back[slot_pairs[:, k]].astype(jnp.float32) * own_weights[:, k:k + 1]]
    pallas_call x1, Pallas kernels: 157 us -> 148 us  [exchange(): pl.pallas_call(functools.partial(exchange_kernel, capacity), out_shape=(j...]
    dot_general x0 -> x3, matrix products: none -> 6.66 us  [the longest x2 4.16 us: on_device(): picked = jnp.dot(place, back, preferred_element_type=jnp.float32)]
    scatter x1 -> x0, local copies, waits for them, and re-layouts: 2.45 us -> none  [fill_table(): jnp.full((slots_total,), empty_value, payload.dtype).at[slot_ids]]
  transfers between devices with their start and end apart: 1 -> 1, of which waited for: 0 -> 0; matrix products, arithmetic and copies ran while one was open for 6% -> 4% of each run, Pallas kernels for 0% -> 0%
where the time goes in v2:
time: 172 us
  Pallas kernels  148 us (86%)
  matrix products  8.92 us (5%)
  starting transfers between devices  4.86 us (3%)
  other arithmetic  4.85 us (3%)
  local copies, waits for them, and re-layouts  4.23 us (2%)
    pallas_call x1, Pallas kernels, exchange(): pl.pallas_call(functools.partial(exchange_kernel, capacity), out_shape=(j...  148 us
    ppermute x1, starting transfers between devices, passed_along(): lax.ppermute(value, axis, [(source, source + steps) for source in range(i...  4.86 us
    dot_general x2, matrix products, on_device(): picked = jnp.dot(place, back, preferred_element_type=jnp.float32)  4.16 us
  transfers between devices with their start and end apart: 1, of which 0 were waited for; matrix products, arithmetic and copies ran while one was open for 4% of the time, Pallas kernels for 0%

profile of v2, /device:TPU:0, one launch (start us, length us, event | category | flops | bytes accessed | tf_op | source)
XLA Modules:
  0.0 171.5 jit_solution(9792254835752840577)
XLA Ops:
  0.6 0.0 copy-start
  0.6 0.0 copy-start.3
  0.7 0.0 copy-start.9
  0.7 0.8 slice.43
  1.5 4.9 %collective-permute-start = (bf16[16,256]{1,0:T(8,128)(2,1)S(1)}, bf16[16,256]{1,0:T(8,128)(2,1)S(1)}, u32[]{:S(2)}, u32[]{:S(2)}) collective-permute-start(bf16[16,256]{1,0:T(8,128)(2,1)S(1)} %slice.43), channel_id=1, source_target_pairs={{0,4},{4,8},{8,12},{12,16},{16,20},{20,24},{24,28},{1,5},{5,9},{9,... | collective-permute-start | bytes 24584 | tf_op jit(solution)/shard_map/ppermute | solution.py:16
  6.4 0.7 constant_dynamic-slice_fusion.1
  7.1 0.1 copy.24
  7.2 0.1 eq.85
  7.4 0.1 eq.81
  7.5 1.2 reduce-window.14
  8.7 0.2 slice_reduce_fusion.2
  8.9 0.1 fusion.30
  9.0 0.1 reduce_sum.39
  9.2 0.1 add_add_fusion
  9.3 0.2 slice_reduce_fusion.1
  9.5 0.0 copy-done.3
  9.5 0.3 fusion.1
  9.8 0.0 copy-start.4
  9.8 0.0 copy-done.9
  9.8 2.5 %convolution_convert_fusion = bf16[640,2048]{1,0:T(8,128)(2,1)} fusion(bf16[256,2048]{1,0:T(8,128)(2,1)S(1)} %copy-done.3, f32[2048]{0:T(1024)S(1)} %copy-done.9, f32[256]{0:T(256)S(1)} %add_rsqrt_fusion.1, s32[256]{0:T(256)S(1)} %get-tuple-element.7, s32[256]{0:T(256)S(1)} %get-tuple-element.6), kind=kOutput, calls=%fused_computation | convolution fusion | flops 674988032 | bytes 3681280 | tf_op jit(solution)/shard_map/dot_general | solution.py:494
  12.3 0.8 constant_dynamic-slice_fusion
  13.2 0.0 collective-permute-done
  13.2 0.0 copy-done.4
  13.2 0.1 fusion.27
  13.3 0.7 fusion.6
  14.0 0.0 copy-start.5
  14.0 0.0 copy-start.8
  14.0 0.1 broadcast_add_fusion
  14.1 0.2 copy.23
  14.4 0.0 copy-done
  14.4 0.5 copy-done.5
  14.9 0.0 copy-done.8
  14.9 2.3 %convolution_convert_fusion.1 = bf16[512,2048]{1,0:T(8,128)(2,1)} fusion(bf16[256,2048]{1,0:T(8,128)(2,1)S(1)} %copy-done, f32[528,256]{1,0:T(8,128)S(1)} %get-tuple-element.9, f32[640,256]{1,0:T(8,128)S(1)} %bitcast.43, f32[528,256]{1,0:T(8,128)S(1)} %slice.57, s32[]{:T(128)S(6)} %select_n.15, f32[256]{0:T(256)S(1)} %copy-done.8, ...), kind=kOutput, calls=%fused_computation.1 | convolution fusion | flops 605814784 | bytes 4852740 | tf_op jit(solution)/shard_map/dot_general | solution.py:499
  17.2 147.8 %shard_map.140 = (bf16[8,80,2048]{2,1,0:T(8,128)(2,1)}, f32[128,2048]{1,0:T(8,128)}) custom-call(bf16[8,80,2048]{2,1,0:T(8,128)(2,1)} %bitcast.49, bf16[4,128,2048]{2,1,0:T(8,128)(2,1)} %bitcast.45, bf16[2,2048,256]{2,1,0:T(8,128)(2,1)} %gate_hbm.1, bf16[2,2048,256]{2,1,0:T(8,128)(2,1)} %up_hbm.1, bf16[2,256,2048]{2,1,0:T(8,128)(2,1)} %down_hbm.1), custom_call_target="tpu_custom_call" | custom-call | flops 16106127360 | bytes 5242880 | tf_op jit(solution)/shard_map/pallas_call | solution.py:396
  165.0 0.0 copy-start.1
  165.0 2.9 %convolution_multiply_fusion = f32[256,2048]{1,0:T(8,128)S(1)} fusion(bf16[640,2048]{1,0:T(8,128)(2,1)} %bitcast.40, f32[256]{0:T(256)S(1)} %bitcast.47, s32[256]{0:T(256)S(1)} %get-tuple-element.7), kind=kOutput, calls=%fused_computation.2 | convolution fusion | flops 671776768 | bytes 4720640 | tf_op jit(solution)/shard_map/dot_general | solution.py:512
  167.9 0.0 copy-done.1
  167.9 0.0 copy-start.2
  167.9 0.0 copy-start.6
  167.9 1.2 multiply_reduce_fusion
  169.2 0.0 copy-start.7
  169.2 0.0 copy-done.2
  169.2 0.2 multiply_reduce_fusion.1
  169.4 0.0 copy-done.6
  169.4 1.0 multiply_convert_fusion.1
  170.3 0.0 copy-done.7
  170.3 1.2 multiply_convert_fusion
  (11 shorter events, 0.2 us)
Async XLA Ops:
  0.6 13.7 %copy-start = (bf16[256,2048]{1,0:T(8,128)(2,1)S(1)}, bf16[256,2048]{1,0:T(8,128)(2,1)}, u32[]{:S(2)}) copy-start(bf16[256,2048]{1,0:T(8,128)(2,1)} %param.16) | copy-start | bytes 3145732
  0.6 8.9 %copy-start.3 = (bf16[256,2048]{1,0:T(8,128)(2,1)S(1)}, bf16[256,2048]{1,0:T(8,128)(2,1)}, u32[]{:S(2)}) copy-start(bf16[256,2048]{1,0:T(8,128)(2,1)} %param.18) | copy-start | bytes 3145732
  0.7 9.2 %copy-start.9 = (f32[2048]{0:T(1024)S(1)}, f32[2048]{0:T(1024)}, u32[]{:S(2)}) copy-start(f32[2048]{0:T(1024)} %param.21) | copy-start | bytes 24580
  1.5 11.7 %collective-permute-start = (bf16[16,256]{1,0:T(8,128)(2,1)S(1)}, bf16[16,256]{1,0:T(8,128)(2,1)S(1)}, u32[]{:S(2)}, u32[]{:S(2)}) collective-permute-start(bf16[16,256]{1,0:T(8,128)(2,1)S(1)} %slice.43), channel_id=1, source_target_pairs={{0,4},{4,8},{8,12},{12,16},{16,20},{20,24},{24,28},{1,5},{5,9},{9,... | collective-permute-start | bytes 24584 | tf_op jit(solution)/shard_map/ppermute | solution.py:16
  9.8 3.4 %copy-start.4 = (bf16[512,256]{1,0:T(8,128)(2,1)S(1)}, bf16[512,256]{1,0:T(8,128)(2,1)}, u32[]{:S(2)}) copy-start(bf16[512,256]{1,0:T(8,128)(2,1)} %param.13) | copy-start | bytes 786436
  14.0 0.9 copy-start.5
  14.0 0.9 copy-start.8
  165.0 2.9 %copy-start.1 = (bf16[8,80,2048]{2,1,0:T(8,128)(2,1)S(1)}, bf16[8,80,2048]{2,1,0:T(8,128)(2,1)}, u32[]{:S(2)}) copy-start(bf16[8,80,2048]{2,1,0:T(8,128)(2,1)} %get-tuple-element.5) | copy-start | bytes 7864324
  167.9 1.3 copy-start.2
  167.9 1.4 copy-start.6
  169.2 1.2 copy-start.7
